TPU v7x, 32 devices: a whole 2x2x4 slice. The times are simulated.
32 devices in a mesh: fs: 8 (over z, y), tp: 4 (over x, core).
Axes of the slice: x: 2, y: 2, z: 4, core: 2. Of those that a mesh axis runs over, the one named last changes fastest.
Arguments:
- later_gate: bfloat16 [5120, 5632], P('fs', 'tp'), may hold values from -6 to 6
- later_up: bfloat16 [5120, 5632], P('fs', 'tp'), may hold values from -6 to 6
- early_gate: bfloat16 [5120, 5632], P('fs', 'tp'), may hold values from -6 to 6
- early_up: bfloat16 [5120, 5632], P('fs', 'tp'), may hold values from -6 to 6
- early_cotangent: bfloat16 [5120, 2048], P(('fs', 'tp')), may hold values from -6 to 6
- down_weight: bfloat16 [5632, 2048], P('tp', 'fs'), may hold values from -0.078125 to 0.078125
- grad_running: float32 [5632, 2048], P('tp', 'fs'), may hold values from -224 to 224
Outputs:
- mixed: bfloat16 [5120, 2048], P(('fs', 'tp'))
- gate_grad: bfloat16 [5120, 5632], P('fs', 'tp')
- up_grad: bfloat16 [5120, 5632], P('fs', 'tp')
- grad_total: float32 [5632, 2048], P('tp', 'fs')
All inputs are finite; a program needn't handle non-finite values.
Results may differ from a plain program's by a relative error of at most 0.009.
Values may be sent and summed in bfloat16 or wider, within the bound.
A program may use at most 128 MiB of HBM per device.

v0:
```python
import jax
import jax.numpy as jnp
from jax import lax
from jax.sharding import PartitionSpec as P


def on_device(
    later_gate, later_up, early_gate, early_up, early_cotangent, down_weight, grad_running
):
    later_hidden = (
        jax.nn.silu(later_gate.astype(jnp.float32)) * later_up.astype(jnp.float32)
    ).astype(jnp.bfloat16)
    gate_value = early_gate.astype(jnp.float32)
    up_value = early_up.astype(jnp.float32)
    sigma = jax.nn.sigmoid(gate_value)
    early_hidden = (gate_value * sigma * up_value).astype(jnp.bfloat16)
    cot_rows = lax.all_gather(early_cotangent, "tp", axis=0, tiled=True)
    whole = lax.all_gather(down_weight, "fs", axis=1, tiled=True)
    mixed = lax.psum_scatter(
        jnp.dot(later_hidden, whole, preferred_element_type=jnp.float32).astype(jnp.bfloat16),
        "tp",
        scatter_dimension=0,
        tiled=True,
    )
    hidden_cot = lax.dot_general(
        cot_rows, whole, (((1,), (1,)), ((), ())), preferred_element_type=jnp.float32
    )
    gate_grad = (hidden_cot * up_value * sigma * (1.0 + gate_value * (1.0 - sigma))).astype(
        jnp.bfloat16
    )
    up_grad = (hidden_cot * gate_value * sigma).astype(jnp.bfloat16)
    summed = lax.psum_scatter(
        lax.dot_general(
            cot_rows, early_hidden, (((0,), (0,)), ((), ())), preferred_element_type=jnp.float32
        ),
        "fs",
        scatter_dimension=0,
        tiled=True,
    )
    grad_total = grad_running + summed.T
    return (mixed, gate_grad, up_grad, grad_total)


def solution(mesh):
    placed = (
        P("fs", "tp"),
        P("fs", "tp"),
        P("fs", "tp"),
        P("fs", "tp"),
        P(("fs", "tp"), None),
        P("tp", "fs"),
        P("tp", "fs"),
    )
    return jax.shard_map(
        on_device,
        mesh=mesh,
        in_specs=placed,
        out_specs=(P(("fs", "tp"), None), P("fs", "tp"), P("fs", "tp"), P("tp", "fs")),
        check_vma=False,
    )
```

profile of v0, /device:TPU:0, one launch (start us, length us, event | category | flops | bytes accessed | tf_op | source)
XLA Modules:
  0.0 371.2 jit_solution(2300562633143723769)
XLA Ops:
  7.2 0.0 all-gather.5.cloned.1.call-start
  7.2 0.7 all-gather.5.cloned.1.call-update
  7.9 0.0 all-gather.3.cloned.1.call-start
  7.9 0.7 all-gather.3.cloned.1.call-update
  8.6 0.0 reduce-scatter.5.cloned.1.call-start
  8.7 29.1 %all-gather.5.cloned.1.call-done = bf16[640,2048]{1,0:T(8,128)(2,1)} async-done(((bf16[160,2048]{1,0:T(8,128)(2,1)}), bf16[640,2048]{1,0:T(8,128)(2,1)}) %all-gather.5.cloned.1.call-update) | async-done | bytes 2621456 | tf_op jit(solution)/shard_map/all_gather | solution.py:17
  37.8 12.2 %convolution_bitcast_fusion = f32[2048,1408]{0,1:T(8,128)} fusion(bf16[640,2048]{1,0:T(8,128)(2,1)} %all-gather.5.cloned.1.call-done, bf16[640,1408]{1,0:T(8,128)(2,1)} %param.10, bf16[640,1408]{1,0:T(8,128)(2,1)} %param.9), kind=kOutput, calls=%fused_computation | convolution fusion | flops 3698196480 | bytes 17760256 | tf_op jit(solution)/shard_map/dot_general | solution.py:33
  50.0 0.0 copy-start.1
  50.0 0.0 reduce-scatter.5.cloned.1.call-update
  50.1 0.2 reduce-scatter.3.cloned.1.call-start
  50.3 82.7 %all-gather.3.cloned.1.call-done = bf16[1408,2048]{1,0:T(8,128)(2,1)} async-done(((bf16[1408,256]{1,0:T(8,128)(2,1)}), bf16[1408,2048]{1,0:T(8,128)(2,1)}) %all-gather.3.cloned.1.call-update) | async-done | bytes 5767184 | tf_op jit(solution)/shard_map/all_gather | solution.py:18
  133.0 0.0 copy-done.1
  133.0 9.2 %convolution_convert_fusion = bf16[640,2048]{1,0:T(8,128)(2,1)} fusion(bf16[1408,2048]{1,0:T(8,128)(2,1)} %all-gather.3.cloned.1.call-done, bf16[640,1408]{1,0:T(8,128)(2,1)S(1)} %copy-done.1, bf16[640,1408]{1,0:T(8,128)(2,1)} %param.7), kind=kOutput, calls=%fused_computation.24 | convolution fusion | flops 3699507200 | bytes 11993088 | tf_op jit(solution)/shard_map/dot_general | solution.py:20
  142.2 0.0 reduce-scatter.3.cloned.1.call-update
  142.2 0.0 copy-start
  142.3 12.0 %fusion.13 = (bf16[640,1408]{1,0:T(8,128)(2,1)}, bf16[640,1408]{1,0:T(8,128)(2,1)}) fusion(bf16[640,1408]{1,0:T(8,128)(2,1)} %param.9, bf16[640,1408]{1,0:T(8,128)(2,1)} %param.10, bf16[640,2048]{1,0:T(8,128)(2,1)} %all-gather.5.cloned.1.call-done, bf16[1408,2048]{1,0:T(8,128)(2,1)} %all-gather.3.cloned.1.call-done), kind=kOutput, calls=%fused_computation.22 | convolution fusion | flops 3704504320 | bytes 15597568 | tf_op jit(solution)/shard_map/dot_general | solution.py:25
  154.3 173.8 %reduce-scatter.5.cloned.1.call-done = f32[256,1408]{0,1:T(8,128)} async-done(((f32[2048,1408]{0,1:T(8,128)}), f32[256,1408]{0,1:T(8,128)}) %reduce-scatter.5.cloned.1.call-update) | async-done | bytes 1441808 | tf_op jit(solution)/shard_map/reduce_scatter | solution.py:32
  328.1 0.0 copy-done
  328.1 2.6 bitcast_add_fusion
  330.7 33.9 %reduce-scatter.3.cloned.1.call-done = bf16[160,2048]{1,0:T(8,128)(2,1)} async-done(((bf16[640,2048]{1,0:T(8,128)(2,1)}), bf16[160,2048]{1,0:T(8,128)(2,1)}) %reduce-scatter.3.cloned.1.call-update) | async-done | bytes 655376 | tf_op jit(solution)/shard_map/reduce_scatter | solution.py:19
Async XLA Ops:
  7.2 30.7 %all-gather.5.cloned.1.call-start = ((), (), s32[]{:S(2)}) async-start(), calls=%async_computation.4 | async-start | bytes 3276800 | tf_op jit(solution)/shard_map/all_gather | solution.py:17
  7.9 125.1 %all-gather.3.cloned.1.call-start = ((), (), s32[]{:S(2)}) async-start(), calls=%async_computation.2 | async-start | bytes 6488064 | tf_op jit(solution)/shard_map/all_gather | solution.py:18
  8.6 319.4 %reduce-scatter.5.cloned.1.call-start = ((), (), s32[]{:S(2)}) async-start(), calls=%async_computation.5 | async-start | bytes 12976128 | tf_op jit(solution)/shard_map/reduce_scatter | solution.py:32
  50.0 83.0 %copy-start.1 = (bf16[640,1408]{1,0:T(8,128)(2,1)S(1)}, bf16[640,1408]{1,0:T(8,128)(2,1)}, u32[]{:S(2)}) copy-start(bf16[640,1408]{1,0:T(8,128)(2,1)} %param.8) | copy-start | bytes 5406724
  50.1 314.6 %reduce-scatter.3.cloned.1.call-start = ((), (), s32[]{:S(2)}) async-start(), calls=%async_computation.3 | async-start | bytes 3276800 | tf_op jit(solution)/shard_map/reduce_scatter | solution.py:19
  142.2 185.8 %copy-start = (f32[1408,256]{1,0:T(8,128)S(1)}, f32[1408,256]{1,0:T(8,128)}, u32[]{:S(2)}) copy-start(f32[1408,256]{1,0:T(8,128)} %param.13) | copy-start | bytes 4325380
Sparse Core Ops, SparseCore 0:
  9.5 28.2 all-gather.4
  39.9 93.1 all-gather.2
  136.6 191.4 reduce-scatter.4
  331.1 33.5 reduce-scatter.2
where the time goes:
time: 371 us
  waiting for transfers between devices  321 us (87%)
  matrix products  33.4 us (9%)
  between operations  13.8 us (4%)
    reduce_scatter x1, waiting for transfers between devices, on_device(): lax.psum_scatter(lax.dot_general(cot_rows, early_hidden, (((0,), (0,)), (...  174 us
    all_gather x1, waiting for transfers between devices, on_device(): whole = lax.all_gather(down_weight, 'fs', axis=1, tiled=True)  82.7 us
    reduce_scatter x1, waiting for transfers between devices, on_device(): lax.psum_scatter(jnp.dot(later_hidden, whole, preferred_element_type=jnp....  33.9 us
    all_gather x1, waiting for transfers between devices, on_device(): cot_rows = lax.all_gather(early_cotangent, 'tp', axis=0, tiled=True)  29.1 us
    dot_general x1, matrix products, on_device(): lax.dot_general(cot_rows, early_hidden, (((0,), (0,)), ((), ())), preferr...  12.2 us
    dot_general x1, matrix products, on_device(): lax.dot_general(cot_rows, whole, (((1,), (1,)), ((), ())), preferred_elem...  12 us
    dot_general x1, matrix products, on_device(): jnp.dot(later_hidden, whole, preferred_element_type=jnp.float32)  9.19 us
  transfers between devices with their start and end apart: 4, of which 4 were waited for; matrix products, arithmetic and copies ran while one was open for 10% of the time, Pallas kernels for 0%

commit v1 on v0

v1 whole, which is shorter than its diff:
```python
import functools

import jax
import jax.numpy as jnp
from jax import lax
from jax.experimental import pallas as pl
from jax.experimental.pallas import tpu as pltpu
from jax.sharding import PartitionSpec as P

PAIR = 2
F32, BF16 = jnp.float32, jnp.bfloat16


def by_collectives(
    later_gate, later_up, early_gate, early_up, early_cotangent, down_weight, grad_running
):
    later_hidden = (
        jax.nn.silu(later_gate.astype(F32)) * later_up.astype(F32)
    ).astype(BF16)
    gate_value = early_gate.astype(F32)
    up_value = early_up.astype(F32)
    sigma = jax.nn.sigmoid(gate_value)
    early_hidden = (gate_value * sigma * up_value).astype(BF16)
    cot_rows = lax.all_gather(early_cotangent, "tp", axis=0, tiled=True)
    whole = lax.all_gather(down_weight, "fs", axis=1, tiled=True)
    mixed = lax.psum_scatter(
        jnp.dot(later_hidden, whole, preferred_element_type=F32).astype(BF16),
        "tp",
        scatter_dimension=0,
        tiled=True,
    )
    hidden_cot = lax.dot_general(
        cot_rows, whole, (((1,), (1,)), ((), ())), preferred_element_type=F32
    )
    gate_grad = (hidden_cot * up_value * sigma * (1.0 + gate_value * (1.0 - sigma))).astype(BF16)
    up_grad = (hidden_cot * gate_value * sigma).astype(BF16)
    summed = lax.psum_scatter(
        lax.dot_general(
            cot_rows, early_hidden, (((0,), (0,)), ((), ())), preferred_element_type=F32
        ),
        "fs",
        scatter_dimension=0,
        tiled=True,
    )
    return (mixed, gate_grad, up_grad, grad_running + summed.T)


def kernel(
    fs, n,
    lg_ref, lu_ref, eg_ref, eu_ref, cot_ref, w_ref, gr_ref,
    mixed_ref, gg_ref, ug_ref, gt_ref,
    lg, lu, eg, eu, run, W, C, Cp, He, Hl, Gs, Gr, own_g, Ms, Mr, hc, mixed,
    loc, wup_s, wdn_s, wy_s, w_r, c_s, c_r, cy_s, cy_r, cp_s, cp_r, h_s, h_r, g_s, g_r, m_s, m_r,
):
    Z = fs // PAIR
    T, K = lg.shape
    B = W.shape[2]
    R = T // n
    me_f, me = lax.axis_index("fs"), lax.axis_index("tp")
    z, y = me_f // PAIR, me_f % PAIR
    buddy = {"fs": z * PAIR + 1 - y}

    def remote(src, dst, ss, rs, to):
        return pltpu.make_async_remote_copy(
            src_ref=src, dst_ref=dst, send_sem=ss, recv_sem=rs,
            device_id=to, device_id_type=pl.DeviceIdType.MESH,
        )

    def block(f):
        return pl.ds(pl.multiple_of(f * B, B), B)

    def rows(t):
        return pl.ds(pl.multiple_of(t * R, R), R)

    others_z = [lax.rem(z + k, Z) for k in range(1, Z)]
    others_t = [lax.rem(me + k, n) for k in range(1, n)]

    loads = [
        pltpu.make_async_copy(src, dst, loc.at[i])
        for i, (src, dst) in enumerate((
            (w_ref, W.at[me_f]), (cot_ref, C.at[rows(me), :]), (eg_ref, eg), (eu_ref, eu),
            (lg_ref, lg), (lu_ref, lu), (gr_ref, run),
        ))
    ]
    for copy in loads:
        copy.start()

    barrier = pltpu.get_barrier_semaphore()
    for to in [buddy] + [{"fs": k * PAIR + y} for k in others_z] + [{"tp": t} for t in others_t]:
        pl.semaphore_signal(barrier, inc=1, device_id=to, device_id_type=pl.DeviceIdType.MESH)
    pl.semaphore_wait(barrier, 1 + len(others_z) + len(others_t))

    def up(zz):
        f = zz * PAIR + y
        return remote(W.at[f], W.at[f], wup_s.at[zz], w_r.at[f], {"fs": (z + 1) * PAIR + y})

    def down(zz):
        f = zz * PAIR + y
        return remote(W.at[f], W.at[f], wdn_s.at[zz], w_r.at[f], {"fs": (z - 1) * PAIR + y})

    def across(zz):
        f = zz * PAIR + y
        return remote(W.at[f], W.at[f], wy_s.at[zz], w_r.at[f], buddy)

    def got_w(f):
        remote(W.at[f], W.at[f], wy_s.at[0], w_r.at[f], buddy).wait_recv()

    loads[0].wait()

    @pl.when(z < Z - 1)
    def _():
        up(z).start()

    @pl.when(z > 0)
    def _():
        down(z).start()

    loads[1].wait()
    cy = [
        remote(
            C.at[rows(me), block(k * PAIR + 1 - y)], Cp.at[rows(me), pl.ds(k * B, B)],
            cy_s.at[k], cy_r.at[k], buddy,
        )
        for k in range(Z)
    ]
    for copy in cy:
        copy.start()
    for t in others_t:
        remote(C.at[rows(me), :], C.at[rows(me), :], c_s.at[t], c_r.at[me], {"tp": t}).start()

    step = 32 if T % 32 == 0 else R

    def hidden(g_ref, u_ref, out):
        @pl.loop(0, T // step)
        def _(i):
            at = pl.ds(pl.multiple_of(i * step, step), step)
            g = g_ref[at, :].astype(F32)
            out[at, :] = (g * jax.nn.sigmoid(g) * u_ref[at, :].astype(F32)).astype(BF16)

    loads[2].wait()
    loads[3].wait()
    hidden(eg, eu, He.at[0])
    swap = remote(He.at[0], He.at[1], h_s.at[0], h_r.at[0], buddy)
    swap.start()

    for copy in cy:
        copy.wait_recv()
    for t in others_t:
        remote(Cp.at[rows(me), :], Cp.at[rows(me), :], cp_s.at[t], cp_r.at[me], {"tp": t}).start()

    loads[4].wait()
    loads[5].wait()
    hidden(lg, lu, Hl)

    def m_copy(f, t):
        return remote(
            Ms.at[rows(t), block(f)], Mr.at[me, :, block(f)],
            m_s.at[f * n + t], m_r.at[f * n + me], {"tp": t},
        )

    def mix(f):
        @pl.loop(0, n)
        def _(t):
            part = jnp.dot(Hl[rows(t), :], W[f], preferred_element_type=F32)
            Ms[rows(t), block(f)] = part.astype(BF16)

        for t in others_t:
            m_copy(f, t).start()

    cuts = [(a, min(a + 512, K)) for a in range(0, K, 512)]

    def back(f, first):
        @pl.loop(0, n)
        def _(t):
            c = C[rows(t), block(f)]
            for a, b in cuts:
                term = lax.dot_general(
                    c, W[f, a:b, :], (((1,), (1,)), ((), ())), preferred_element_type=F32
                )
                hc[rows(t), a:b] = term if first else hc[rows(t), a:b] + term

    def in_order(body):
        @pl.loop(0, 2 * Z - 1)
        def _(c):
            d = (c + 1) // 2
            zz = jnp.where(c % 2 == 1, z - d, z + d)

            @pl.when((zz >= 0) & (zz < Z))
            def _():
                body(c, zz)

    def relay(c, zz):
        @pl.when(c > 0)
        def _():
            got_w(zz * PAIR + y)

        @pl.when((c > 0) & (zz < z) & (z < Z - 1))
        def _():
            up(zz).start()

        @pl.when((c > 0) & (zz > z) & (z > 0))
        def _():
            down(zz).start()

        across(zz).start()
        mix(zz * PAIR + y)

    in_order(relay)

    for t in others_t:
        remote(C.at[rows(t), :], C.at[rows(t), :], c_s.at[t], c_r.at[t], {"tp": t}).wait_recv()
        remote(Cp.at[rows(t), :], Cp.at[rows(t), :], cp_s.at[t], cp_r.at[t], {"tp": t}).wait_recv()
    swap.wait_recv()
    over_rows = (((0,), (0,)), ((), ()))

    @pl.loop(0, K // 128)
    def _(i):
        at = pl.ds(pl.multiple_of(i * 128, 128), 128)
        mine, theirs = He[0, :, at], He[1, :, at]
        for k in range(Z):
            zz = lax.rem(z + k, Z)
            term = lax.dot_general(
                mine, C[:, block(zz * PAIR + y)], over_rows, preferred_element_type=F32
            ) + lax.dot_general(theirs, Cp[:, block(zz)], over_rows, preferred_element_type=F32)
            if k == 0:
                own_g[at, :] = term
            else:
                Gs[zz, at, :] = term.astype(BF16)

    def g_copy(zz):
        return remote(Gs.at[zz], Gr.at[z], g_s.at[zz], g_r.at[z], {"fs": zz * PAIR + y})

    for zz in others_z:
        g_copy(zz).start()

    back(z * PAIR + y, True)
    in_order(lambda c, zz: pl.when(c > 0)(lambda: back(zz * PAIR + y, False)))

    def partner(c, zz):
        f = zz * PAIR + 1 - y
        got_w(f)
        mix(f)
        back(f, False)

    in_order(partner)

    outs = []

    @pl.loop(0, T // step)
    def _(i):
        at = pl.ds(pl.multiple_of(i * step, step), step)
        g, u, h = eg[at, :].astype(F32), eu[at, :].astype(F32), hc[at, :]
        s = jax.nn.sigmoid(g)
        lg[at, :] = (h * u * s * (1.0 + g * (1.0 - s))).astype(BF16)
        lu[at, :] = (h * g * s).astype(BF16)

    outs.append(pltpu.make_async_copy(lg, gg_ref, loc.at[7]))
    outs.append(pltpu.make_async_copy(lu, ug_ref, loc.at[8]))
    for copy in outs:
        copy.start()

    for zz in others_z:
        remote(Gs.at[zz], Gr.at[zz], g_s.at[zz], g_r.at[zz], buddy).wait_recv()
    loads[6].wait()

    @pl.loop(0, K // 128)
    def _(i):
        at = pl.ds(pl.multiple_of(i * 128, 128), 128)
        total = own_g[at, :]
        for zz in others_z:
            total = total + Gr[zz, at, :].astype(F32)
        own_g[at, :] = run[at, :] + total

    outs.append(pltpu.make_async_copy(own_g, gt_ref, loc.at[9]))
    outs[-1].start()

    @pl.loop(0, fs)
    def _(f):
        for t in others_t:
            remote(
                Ms.at[rows(t), block(f)], Mr.at[t, :, block(f)],
                m_s.at[f * n + t], m_r.at[f * n + t], {"tp": t},
            ).wait_recv()
        total = Ms[rows(me), block(f)].astype(F32)
        for t in others_t:
            total = total + Mr[t, :, block(f)].astype(F32)
        mixed[:, block(f)] = total.astype(BF16)

    outs.append(pltpu.make_async_copy(mixed, mixed_ref, loc.at[10]))
    outs[-1].start()

    def sent(c, zz):
        @pl.when((zz <= z) & (z < Z - 1))
        def _():
            up(zz).wait_send()

        @pl.when((zz >= z) & (z > 0))
        def _():
            down(zz).wait_send()

        across(zz).wait_send()

    in_order(sent)
    for copy in cy:
        copy.wait_send()
    for t in others_t:
        remote(C.at[rows(me), :], C.at[rows(me), :], c_s.at[t], c_r.at[me], {"tp": t}).wait_send()
        remote(Cp.at[rows(me), :], Cp.at[rows(me), :], cp_s.at[t], cp_r.at[me], {"tp": t}).wait_send()
    swap.wait_send()
    for zz in others_z:
        g_copy(zz).wait_send()

    @pl.loop(0, fs)
    def _(f):
        for t in others_t:
            m_copy(f, t).wait_send()

    for copy in outs:
        copy.wait()


def by_kernel(fs, n, *args):
    later_gate, cot, weight = args[0], args[4], args[5]
    T, K = later_gate.shape
    R, D = cot.shape
    B = weight.shape[1]
    Z = fs // PAIR
    sem = pltpu.SemaphoreType.DMA
    anywhere = pl.BlockSpec(memory_space=pl.ANY)
    return pl.pallas_call(
        functools.partial(kernel, fs, n),
        out_shape=(
            jax.ShapeDtypeStruct((R, D), BF16),
            jax.ShapeDtypeStruct((T, K), BF16),
            jax.ShapeDtypeStruct((T, K), BF16),
            jax.ShapeDtypeStruct((K, B), F32),
        ),
        in_specs=[anywhere] * 7,
        out_specs=(anywhere,) * 4,
        scratch_shapes=[
            pltpu.VMEM((T, K), BF16), pltpu.VMEM((T, K), BF16),
            pltpu.VMEM((T, K), BF16), pltpu.VMEM((T, K), BF16),
            pltpu.VMEM((K, B), F32),
            pltpu.VMEM((fs, K, B), BF16),
            pltpu.VMEM((T, D), BF16),
            pltpu.VMEM((T, Z * B), BF16),
            pltpu.VMEM((2, T, K), BF16),
            pltpu.VMEM((T, K), BF16),
            pltpu.VMEM((Z, K, B), BF16), pltpu.VMEM((Z, K, B), BF16),
            pltpu.VMEM((K, B), F32),
            pltpu.VMEM((T, D), BF16),
            pltpu.VMEM((n, R, D), BF16),
            pltpu.VMEM((T, K), F32),
            pltpu.VMEM((R, D), BF16),
            sem((11,)),
            sem((Z,)), sem((Z,)), sem((Z,)), sem((fs,)),
            sem((n,)), sem((n,)), sem((Z,)), sem((Z,)), sem((n,)), sem((n,)),
            sem((1,)), sem((1,)), sem((Z,)), sem((Z,)),
            sem((fs * n,)), sem((fs * n,)),
        ],
        compiler_params=pltpu.CompilerParams(
            collective_id=0, has_side_effects=True, vmem_limit_bytes=62 * 2**20
        ),
    )(*args)


def solution(mesh):
    fs, n = mesh.shape["fs"], mesh.shape["tp"]

    def on_device(*args):
        T, K = args[0].shape
        B = args[5].shape[1]
        if fs % PAIR == 0 and fs >= 4 and B % 128 == 0 and K % 128 == 0 and (T // n) % 32 == 0:
            return by_kernel(fs, n, *args)
        return by_collectives(*args)

    placed = (
        P("fs", "tp"),
        P("fs", "tp"),
        P("fs", "tp"),
        P("fs", "tp"),
        P(("fs", "tp"), None),
        P("tp", "fs"),
        P("tp", "fs"),
    )
    return jax.shard_map(
        on_device,
        mesh=mesh,
        in_specs=placed,
        out_specs=(P(("fs", "tp"), None), P("fs", "tp"), P("fs", "tp"), P("tp", "fs")),
        check_vma=False,
    )
```

time: 371 us -> 132 us (0.36)
  waiting for transfers between devices: 321 us -> 0 us
  Pallas kernels: 0 us -> 123 us
  matrix products: 33.4 us -> 0 us
  between operations: 13.8 us -> 0.64 us
  local copies, waits for them, and re-layouts: 0.01 us -> 8.07 us
    reduce_scatter x2 -> x0, waiting for transfers between devices: 208 us -> none  [the longest x1 174 us: on_device(): lax.psum_scatter(lax.dot_general(cot_rows, early_hidden, (((0,), (0,)), (...]
    pallas_call x0 -> x1, Pallas kernels: none -> 123 us  [by_kernel(): pl.pallas_call(functools.partial(kernel, fs, n), out_shape=(jax.ShapeDtyp...]
    all_gather x2 -> x0, waiting for transfers between devices: 112 us -> none  [the longest x1 82.7 us: on_device(): whole = lax.all_gather(down_weight, 'fs', axis=1, tiled=True)]
    dot_general x3 -> x0, matrix products: 33.4 us -> none  [the longest x1 12.2 us: on_device(): lax.dot_general(cot_rows, early_hidden, (((0,), (0,)), ((), ())), preferr...]
    unnamed x4 -> x8, local copies, waits for them, and re-layouts: 0.01 us -> 8.07 us
  transfers between devices with their start and end apart: 4 -> 0, of which waited for: 4 -> 0; matrix products, arithmetic and copies ran while one was open for 10% -> 0% of each run, Pallas kernels for 0% -> 0%
where the time goes in v1:
time: 132 us; the launch traced here: 131 us
  Pallas kernels  123 us (93%)
  local copies, waits for them, and re-layouts  8.07 us (6%)
    pallas_call x1, Pallas kernels, by_kernel(): pl.pallas_call(functools.partial(kernel, fs, n), out_shape=(jax.ShapeDtyp...  123 us
    unnamed x8, local copies, waits for them, and re-layouts  8.07 us

profile of v1, /device:TPU:0, one launch (start us, length us, event | category | flops | bytes accessed | tf_op | source)
XLA Modules:
  0.0 131.4 jit_solution(1680869553162726222)
XLA Ops:
  0.6 122.7 %shard_map.102 = (bf16[160,2048]{1,0:T(8,128)(2,1)}, bf16[640,1408]{1,0:T(8,128)(2,1)}, bf16[640,1408]{1,0:T(8,128)(2,1)}, f32[1408,256]{1,0:T(8,128)}) custom-call(bf16[640,1408]{1,0:T(8,128)(2,1)} %lg_ref.1, bf16[640,1408]{1,0:T(8,128)(2,1)} %lu_ref.1, bf16[640,1408]{1,0:T(8,128)(2,1)} %eg_ref.1, bf16[640,1408]{1,0:T(8,128)(2,1)} %eu_ref.1, ...), custom_call_target="tpu_custom_call" | custom-call | tf_op jit(solution)/shard_map/pallas_call | solution.py:330
  123.3 2.0 %copy.15 = bf16[160,2048]{1,0:T(8,128)(2,1)} copy(bf16[160,2048]{1,0:T(8,128)(2,1)} %get-tuple-element.8) | data formatting | bytes 1310720
  125.3 0.0 copy-start
  125.3 3.0 %copy.16 = bf16[640,1408]{1,0:T(8,128)(2,1)} copy(bf16[640,1408]{1,0:T(8,128)(2,1)} %get-tuple-element.9) | data formatting | bytes 3604480
  128.3 0.0 copy-done
  128.3 0.0 copy-start.1
  128.3 1.2 copy.17
  129.5 0.8 copy-done.1
  130.3 1.1 copy.18
Async XLA Ops:
  125.3 3.0 %copy-start = (bf16[640,1408]{1,0:T(8,128)(2,1)S(1)}, bf16[640,1408]{1,0:T(8,128)(2,1)}, u32[]{:S(2)}) copy-start(bf16[640,1408]{1,0:T(8,128)(2,1)} %get-tuple-element.10) | copy-start | bytes 5406724
  128.3 2.0 %copy-start.1 = (f32[1408,256]{1,0:T(8,128)S(1)}, f32[1408,256]{1,0:T(8,128)}, u32[]{:S(2)}) copy-start(f32[1408,256]{1,0:T(8,128)} %get-tuple-element.11) | copy-start | bytes 4325380

commit v2 on v1

--- a/solution.py
+++ b/solution.py
@@ -45,17 +45,24 @@
     return (mixed, gate_grad, up_grad, grad_running + summed.T)
 
 
+def parts_of(K):
+    size = -(-(K // 128) // 4) * 128
+    return [(a, min(a + size, K)) for a in range(0, K, size)]
+
+
 def kernel(
     fs, n,
     lg_ref, lu_ref, eg_ref, eu_ref, cot_ref, w_ref, gr_ref,
     mixed_ref, gg_ref, ug_ref, gt_ref,
     lg, lu, eg, eu, run, W, C, Cp, He, Hl, Gs, Gr, own_g, Ms, Mr, hc, mixed,
     loc, wup_s, wdn_s, wy_s, w_r, c_s, c_r, cy_s, cy_r, cp_s, cp_r, h_s, h_r, g_s, g_r, m_s, m_r,
+    wb_s, wb_r, wbu_s, wbd_s,
 ):
     Z = fs // PAIR
     T, K = lg.shape
     B = W.shape[2]
     R = T // n
+    early = max(K * 3 // 22 // 64, 1) * 64
     me_f, me = lax.axis_index("fs"), lax.axis_index("tp")
     z, y = me_f // PAIR, me_f % PAIR
     buddy = {"fs": z * PAIR + 1 - y}
@@ -98,9 +105,22 @@
         f = zz * PAIR + y
         return remote(W.at[f], W.at[f], wdn_s.at[zz], w_r.at[f], {"fs": (z - 1) * PAIR + y})
 
-    def across(zz):
-        f = zz * PAIR + y
-        return remote(W.at[f], W.at[f], wy_s.at[zz], w_r.at[f], buddy)
+    def across(zz, source=y):
+        f = zz * PAIR + source
+        part = W.at[f, early:, :]
+        return remote(part, part, wy_s.at[zz], w_r.at[f], buddy)
+
+    def first_across():
+        part = W.at[me_f, :early, :]
+        return remote(part, part, wb_s.at[0], wb_r.at[z], buddy)
+
+    def first_up(zz):
+        part = W.at[zz * PAIR + 1 - y, :early, :]
+        return remote(part, part, wbu_s.at[zz], wb_r.at[zz], {"fs": (z + 1) * PAIR + y})
+
+    def first_down(zz):
+        part = W.at[zz * PAIR + 1 - y, :early, :]
+        return remote(part, part, wbd_s.at[zz], wb_r.at[zz], {"fs": (z - 1) * PAIR + y})
 
     def got_w(f):
         remote(W.at[f], W.at[f], wy_s.at[0], w_r.at[f], buddy).wait_recv()
@@ -115,6 +135,7 @@
     def _():
         down(z).start()
 
+    first_across().start()
     loads[1].wait()
     cy = [
         remote(
@@ -125,32 +146,50 @@
     ]
     for copy in cy:
         copy.start()
-    for t in others_t:
-        remote(C.at[rows(me), :], C.at[rows(me), :], c_s.at[t], c_r.at[me], {"tp": t}).start()
-
+
+    def c_copy(t, f, source):
+        part = C.at[rows(source), block(f)]
+        return remote(part, part, c_s.at[t * fs + f], c_r.at[source * fs + f], {"tp": t})
+
+    def c_send(side):
+        for k in range(Z):
+            for t in others_t:
+                c_copy(t, k * PAIR + side, me).start()
+
+    def c_wait(side):
+        for k in range(Z):
+            for t in others_t:
+                c_copy(t, k * PAIR + side, t).wait_recv()
+
+    c_send(y)
     step = 32 if T % 32 == 0 else R
 
-    def hidden(g_ref, u_ref, out):
+    def hidden(g_ref, u_ref, out, a, b):
         @pl.loop(0, T // step)
         def _(i):
             at = pl.ds(pl.multiple_of(i * step, step), step)
-            g = g_ref[at, :].astype(F32)
-            out[at, :] = (g * jax.nn.sigmoid(g) * u_ref[at, :].astype(F32)).astype(BF16)
+            g = g_ref[at, a:b].astype(F32)
+            out[at, a:b] = (g * jax.nn.sigmoid(g) * u_ref[at, a:b].astype(F32)).astype(BF16)
 
     loads[2].wait()
     loads[3].wait()
-    hidden(eg, eu, He.at[0])
-    swap = remote(He.at[0], He.at[1], h_s.at[0], h_r.at[0], buddy)
-    swap.start()
+    swaps = []
+    for q, (a, b) in enumerate(parts_of(K)):
+        hidden(eg, eu, He.at[0], a, b)
+        swaps.append(
+            remote(He.at[0, :, a:b], He.at[1, :, a:b], h_s.at[q], h_r.at[q], buddy)
+        )
+        swaps[-1].start()
 
     for copy in cy:
         copy.wait_recv()
     for t in others_t:
         remote(Cp.at[rows(me), :], Cp.at[rows(me), :], cp_s.at[t], cp_r.at[me], {"tp": t}).start()
+    c_send(1 - y)
 
     loads[4].wait()
     loads[5].wait()
-    hidden(lg, lu, Hl)
+    hidden(lg, lu, Hl, 0, K)
 
     def m_copy(f, t):
         return remote(
@@ -179,8 +218,8 @@
                 )
                 hc[rows(t), a:b] = term if first else hc[rows(t), a:b] + term
 
-    def in_order(body):
-        @pl.loop(0, 2 * Z - 1)
+    def in_order(body, first=0, end=2 * Z - 1):
+        @pl.loop(first, end)
         def _(c):
             d = (c + 1) // 2
             zz = jnp.where(c % 2 == 1, z - d, z + d)
@@ -202,43 +241,69 @@
         def _():
             down(zz).start()
 
+        part = W.at[zz * PAIR + 1 - y, :early, :]
+        remote(part, part, wb_s.at[0], wb_r.at[zz], buddy).wait_recv()
+
+        @pl.when((zz <= z) & (z < Z - 1))
+        def _():
+            first_up(zz).start()
+
+        @pl.when((zz >= z) & (z > 0))
+        def _():
+            first_down(zz).start()
+
         across(zz).start()
         mix(zz * PAIR + y)
 
-    in_order(relay)
-
+    over_rows = (((0,), (0,)), ((), ()))
+
+    def g_copy(q, zz, source):
+        a, b = parts_of(K)[q]
+        return remote(
+            Gs.at[zz, a:b, :], Gr.at[source, a:b, :],
+            g_s.at[q * Z + zz], g_r.at[q * Z + source], {"fs": zz * PAIR + y},
+        )
+
+    def terms(q):
+        swaps[q].wait_recv()
+        a, b = parts_of(K)[q]
+
+        @pl.loop(a // 128, b // 128)
+        def _(i):
+            at = pl.ds(pl.multiple_of(i * 128, 128), 128)
+            mine, theirs = He[0, :, at], He[1, :, at]
+            for k in range(Z):
+                zz = lax.rem(z + k, Z)
+                term = lax.dot_general(
+                    mine, C[:, block(zz * PAIR + y)], over_rows, preferred_element_type=F32
+                ) + lax.dot_general(theirs, Cp[:, block(zz)], over_rows, preferred_element_type=F32)
+                if k == 0:
+                    own_g[at, :] = term
+                else:
+                    Gs[zz, at, :] = term.astype(BF16)
+
+        for zz in others_z:
+            g_copy(q, zz, z).start()
+
+    parts = len(parts_of(K))
+    near = min(5, 2 * Z - 1)
+    in_order(relay, 0, near)
+    c_wait(y)
     for t in others_t:
-        remote(C.at[rows(t), :], C.at[rows(t), :], c_s.at[t], c_r.at[t], {"tp": t}).wait_recv()
         remote(Cp.at[rows(t), :], Cp.at[rows(t), :], cp_s.at[t], cp_r.at[t], {"tp": t}).wait_recv()
-    swap.wait_recv()
-    over_rows = (((0,), (0,)), ((), ()))
-
-    @pl.loop(0, K // 128)
-    def _(i):
-        at = pl.ds(pl.multiple_of(i * 128, 128), 128)
-        mine, theirs = He[0, :, at], He[1, :, at]
-        for k in range(Z):
-            zz = lax.rem(z + k, Z)
-            term = lax.dot_general(
-                mine, C[:, block(zz * PAIR + y)], over_rows, preferred_element_type=F32
-            ) + lax.dot_general(theirs, Cp[:, block(zz)], over_rows, preferred_element_type=F32)
-            if k == 0:
-                own_g[at, :] = term
-            else:
-                Gs[zz, at, :] = term.astype(BF16)
-
-    def g_copy(zz):
-        return remote(Gs.at[zz], Gr.at[z], g_s.at[zz], g_r.at[z], {"fs": zz * PAIR + y})
-
-    for zz in others_z:
-        g_copy(zz).start()
+    for q in range(parts // 2):
+        terms(q)
+    in_order(relay, near)
+    for q in range(parts // 2, parts):
+        terms(q)
+    c_wait(1 - y)
 
     back(z * PAIR + y, True)
     in_order(lambda c, zz: pl.when(c > 0)(lambda: back(zz * PAIR + y, False)))
 
     def partner(c, zz):
         f = zz * PAIR + 1 - y
-        got_w(f)
+        across(zz, 1 - y).wait_recv()
         mix(f)
         back(f, False)
 
@@ -246,21 +311,24 @@
 
     outs = []
 
-    @pl.loop(0, T // step)
-    def _(i):
-        at = pl.ds(pl.multiple_of(i * step, step), step)
-        g, u, h = eg[at, :].astype(F32), eu[at, :].astype(F32), hc[at, :]
-        s = jax.nn.sigmoid(g)
-        lg[at, :] = (h * u * s * (1.0 + g * (1.0 - s))).astype(BF16)
-        lu[at, :] = (h * g * s).astype(BF16)
-
-    outs.append(pltpu.make_async_copy(lg, gg_ref, loc.at[7]))
-    outs.append(pltpu.make_async_copy(lu, ug_ref, loc.at[8]))
-    for copy in outs:
-        copy.start()
-
-    for zz in others_z:
-        remote(Gs.at[zz], Gr.at[zz], g_s.at[zz], g_r.at[zz], buddy).wait_recv()
+    for t in range(n):
+        @pl.loop(t * R // step, (t + 1) * R // step)
+        def _(i):
+            at = pl.ds(pl.multiple_of(i * step, step), step)
+            g, u, h = eg[at, :].astype(F32), eu[at, :].astype(F32), hc[at, :]
+            s = jax.nn.sigmoid(g)
+            lg[at, :] = (h * u * s * (1.0 + g * (1.0 - s))).astype(BF16)
+            lu[at, :] = (h * g * s).astype(BF16)
+
+        at = pl.ds(t * R, R)
+        outs.append(pltpu.make_async_copy(lg.at[at, :], gg_ref.at[at, :], loc.at[9 + 2 * t]))
+        outs.append(pltpu.make_async_copy(lu.at[at, :], ug_ref.at[at, :], loc.at[10 + 2 * t]))
+        outs[-2].start()
+        outs[-1].start()
+
+    for q in range(parts):
+        for zz in others_z:
+            g_copy(q, zz, zz).wait_recv()
     loads[6].wait()
 
     @pl.loop(0, K // 128)
@@ -271,7 +339,7 @@
             total = total + Gr[zz, at, :].astype(F32)
         own_g[at, :] = run[at, :] + total
 
-    outs.append(pltpu.make_async_copy(own_g, gt_ref, loc.at[9]))
+    outs.append(pltpu.make_async_copy(own_g, gt_ref, loc.at[7]))
     outs[-1].start()
 
     @pl.loop(0, fs)
@@ -286,29 +354,35 @@
             total = total + Mr[t, :, block(f)].astype(F32)
         mixed[:, block(f)] = total.astype(BF16)
 
-    outs.append(pltpu.make_async_copy(mixed, mixed_ref, loc.at[10]))
+    outs.append(pltpu.make_async_copy(mixed, mixed_ref, loc.at[8]))
     outs[-1].start()
 
     def sent(c, zz):
         @pl.when((zz <= z) & (z < Z - 1))
         def _():
             up(zz).wait_send()
+            first_up(zz).wait_send()
 
         @pl.when((zz >= z) & (z > 0))
         def _():
             down(zz).wait_send()
+            first_down(zz).wait_send()
 
         across(zz).wait_send()
 
     in_order(sent)
+    first_across().wait_send()
     for copy in cy:
         copy.wait_send()
     for t in others_t:
-        remote(C.at[rows(me), :], C.at[rows(me), :], c_s.at[t], c_r.at[me], {"tp": t}).wait_send()
+        for f in range(fs):
+            c_copy(t, f, me).wait_send()
         remote(Cp.at[rows(me), :], Cp.at[rows(me), :], cp_s.at[t], cp_r.at[me], {"tp": t}).wait_send()
-    swap.wait_send()
-    for zz in others_z:
-        g_copy(zz).wait_send()
+    for copy in swaps:
+        copy.wait_send()
+    for q in range(parts):
+        for zz in others_z:
+            g_copy(q, zz, z).wait_send()
 
     @pl.loop(0, fs)
     def _(f):
@@ -325,6 +399,7 @@
     R, D = cot.shape
     B = weight.shape[1]
     Z = fs // PAIR
+    parts = len(parts_of(K))
     sem = pltpu.SemaphoreType.DMA
     anywhere = pl.BlockSpec(memory_space=pl.ANY)
     return pl.pallas_call(
@@ -352,11 +427,12 @@
             pltpu.VMEM((n, R, D), BF16),
             pltpu.VMEM((T, K), F32),
             pltpu.VMEM((R, D), BF16),
-            sem((11,)),
+            sem((9 + 2 * n,)),
             sem((Z,)), sem((Z,)), sem((Z,)), sem((fs,)),
-            sem((n,)), sem((n,)), sem((Z,)), sem((Z,)), sem((n,)), sem((n,)),
-            sem((1,)), sem((1,)), sem((Z,)), sem((Z,)),
+            sem((n * fs,)), sem((n * fs,)), sem((Z,)), sem((Z,)), sem((n,)), sem((n,)),
+            sem((parts,)), sem((parts,)), sem((parts * Z,)), sem((parts * Z,)),
             sem((fs * n,)), sem((fs * n,)),
+            sem((1,)), sem((Z,)), sem((Z,)), sem((Z,)),
         ],
         compiler_params=pltpu.CompilerParams(
             collective_id=0, has_side_effects=True, vmem_limit_bytes=62 * 2**20

time: 132 us -> 126 us (0.955)
  Pallas kernels: 123 us -> 117 us
    pallas_call x1, Pallas kernels: 123 us -> 117 us  [by_kernel(): pl.pallas_call(functools.partial(kernel, fs, n), out_shape=(jax.ShapeDtyp...]
where the time goes in v2:
time: 126 us; the launch traced here: 125 us
  Pallas kernels  117 us (93%)
  local copies, waits for them, and re-layouts  8.07 us (6%)
    pallas_call x1, Pallas kernels, by_kernel(): pl.pallas_call(functools.partial(kernel, fs, n), out_shape=(jax.ShapeDtyp...  117 us
    unnamed x8, local copies, waits for them, and re-layouts  8.07 us

profile of v2, /device:TPU:0, one launch (start us, length us, event | category | flops | bytes accessed | tf_op | source)
XLA Modules:
  0.0 125.4 jit_solution(507412567779341872)
XLA Ops:
  0.6 116.7 %shard_map.102 = (bf16[160,2048]{1,0:T(8,128)(2,1)}, bf16[640,1408]{1,0:T(8,128)(2,1)}, bf16[640,1408]{1,0:T(8,128)(2,1)}, f32[1408,256]{1,0:T(8,128)}) custom-call(bf16[640,1408]{1,0:T(8,128)(2,1)} %lg_ref.1, bf16[640,1408]{1,0:T(8,128)(2,1)} %lu_ref.1, bf16[640,1408]{1,0:T(8,128)(2,1)} %eg_ref.1, bf16[640,1408]{1,0:T(8,128)(2,1)} %eu_ref.1, ...), custom_call_target="tpu_custom_call" | custom-call | tf_op jit(solution)/shard_map/pallas_call | solution.py:405
  117.3 2.0 %copy.15 = bf16[160,2048]{1,0:T(8,128)(2,1)} copy(bf16[160,2048]{1,0:T(8,128)(2,1)} %get-tuple-element.8) | data formatting | bytes 1310720
  119.3 0.0 copy-start
  119.3 3.0 %copy.16 = bf16[640,1408]{1,0:T(8,128)(2,1)} copy(bf16[640,1408]{1,0:T(8,128)(2,1)} %get-tuple-element.9) | data formatting | bytes 3604480
  122.3 0.0 copy-done
  122.3 0.0 copy-start.1
  122.3 1.2 copy.17
  123.5 0.8 copy-done.1
  124.3 1.1 copy.18
Async XLA Ops:
  119.3 3.0 %copy-start = (bf16[640,1408]{1,0:T(8,128)(2,1)S(1)}, bf16[640,1408]{1,0:T(8,128)(2,1)}, u32[]{:S(2)}) copy-start(bf16[640,1408]{1,0:T(8,128)(2,1)} %get-tuple-element.10) | copy-start | bytes 5406724
  122.3 2.0 %copy-start.1 = (f32[1408,256]{1,0:T(8,128)S(1)}, f32[1408,256]{1,0:T(8,128)}, u32[]{:S(2)}) copy-start(f32[1408,256]{1,0:T(8,128)} %get-tuple-element.11) | copy-start | bytes 4325380
